TPU v7x, 32 devices: a whole 2x2x4 slice. The times are simulated.
32 devices in a mesh: sp: 4 (over z), fs: 4 (over y, x), tp: 2 (over core).
Axes of the slice: x: 2, y: 2, z: 4, core: 2. Of those that a mesh axis runs over, the one named last changes fastest.
Arguments:
- tokens: bfloat16 [4, 3072, 2048], P('fs', 'sp'), may hold values from -6 to 6
- norm_gain: float32 [2048], replicated, may hold values from 0.1 to 1.9
- query_weight: bfloat16 [2048, 512], P(('sp', 'fs'), 'tp'), may hold values from -0.125 to 0.125
- key_weight: bfloat16 [2048, 512], P(('sp', 'fs'), 'tp'), may hold values from -0.125 to 0.125
- value_weight: bfloat16 [2048, 1024], P(('sp', 'fs'), 'tp'), may hold values from -0.125 to 0.125
- gate_weight: bfloat16 [2048, 1024], P(('sp', 'fs'), 'tp'), may hold values from -0.125 to 0.125
- conv_b_weight: bfloat16 [2048, 1024], P(('sp', 'fs'), 'tp'), may hold values from -0.125 to 0.125
- conv_c_weight: bfloat16 [2048, 1024], P(('sp', 'fs'), 'tp'), may hold values from -0.125 to 0.125
- conv_in_weight: bfloat16 [2048, 1024], P(('sp', 'fs'), 'tp'), may hold values from -0.125 to 0.125
- conv_kernel: float32 [3, 1024], P(None, 'tp'), may hold values from -3.5 to 3.5
- out_ret_weight: bfloat16 [2048, 1024], P(('sp', 'fs'), 'tp'), may hold values from -0.125 to 0.125
- out_conv_weight: bfloat16 [2048, 1024], P(('sp', 'fs'), 'tp'), may hold values from -0.125 to 0.125
- log_decay: float32 [4, 8, 3072], P('fs', 'tp', 'sp'), may hold values from -3 to 0, as said below
Outputs:
- mixed: bfloat16 [4, 3072, 2048], P('fs', ('sp', 'tp'))
Inputs may be any that keep to these rules, and one draw needn't show every extreme that they name: log_decay is never positive.
All inputs are finite; a program needn't handle non-finite values.
Results may differ from a plain program's by a relative error of at most 0.02.
Values may be sent and summed in bfloat16 or wider, within the bound.
A program may use at most 64 MiB of HBM per device.

v0:
```python
import jax
import jax.numpy as jnp
from jax import lax
from jax.sharding import PartitionSpec as P

KEY_DIM = 64
VALUE_DIM = 128
CONV_TAPS = 3
BLOCK_LEN = 128


EPSILON = 1e-06
ROPE_BASE = 10000.0


def entering(x, axis, combine, identity):
    length, here = (lax.axis_size(axis), lax.axis_index(axis))
    everything = jax.tree.map(
        lambda part, kind: lax.all_gather(part.astype(kind), axis), x, (jnp.bfloat16, jnp.bfloat16)
    )
    start = jax.tree.map(
        lambda part, zero: jnp.broadcast_to(jnp.asarray(zero, part.dtype), part.shape), x, identity
    )

    def lap(k, before):
        reached = k < here
        new = combine(
            before, jax.tree.map(lambda part, own: part[k].astype(own.dtype), everything, x)
        )
        return jax.tree.map(lambda a, b: jnp.where(reached, a, b), new, before)

    return lax.fori_loop(0, length, lap, start)


def passed_along(value, axis, steps):
    count = lax.axis_size(axis)
    first, last = (max(0, -steps), min(count, count - steps))
    return lax.ppermute(value, axis, [(source, source + steps) for source in range(first, last)])


def rotate(values, token_ordinal):
    half_dim = values.shape[-1] // 2
    frequency = 1.0 / ROPE_BASE ** jnp.linspace(0.0, 1.0, half_dim, dtype=jnp.float32)
    angles = token_ordinal[:, None] * frequency[None, :]
    cosine_table = jnp.cos(angles)[:, None, :]
    sine_table = jnp.sin(angles)[:, None, :]
    first = values[..., :half_dim].astype(jnp.float32)
    second = values[..., half_dim:].astype(jnp.float32)
    return jnp.concatenate(
        [first * cosine_table - second * sine_table, first * sine_table + second * cosine_table],
        axis=-1,
    )


def make_adder(normed, contracted, pieces):
    updated = []
    for member in range(len(pieces)):
        portion = pieces[member]
        if member < contracted:
            updated.append(jnp.dot(normed, portion, preferred_element_type=jnp.float32))
        else:
            updated.append(portion)
    return tuple(updated)


def retention_local(projections, decays, token_ordinal):
    tok_rows = token_ordinal.shape[0]
    head_count = decays.shape[0]
    blocks = tok_rows // BLOCK_LEN
    query_raw = projections[0].reshape(tok_rows, head_count, KEY_DIM)
    key_raw = projections[1].reshape(tok_rows, head_count, KEY_DIM)
    queries = rotate(query_raw, token_ordinal).astype(jnp.bfloat16)
    lookup_matrix_lines = (rotate(key_raw, token_ordinal) * KEY_DIM ** (-0.5)).astype(jnp.bfloat16)
    value_proj = projections[2].reshape(tok_rows, head_count, VALUE_DIM)

    def split_blocks(array):
        shaped = array.reshape(blocks, BLOCK_LEN, head_count, array.shape[-1])
        return jnp.transpose(shaped, (0, 2, 1, 3))

    query_blocks = split_blocks(queries)
    key_blocks = split_blocks(lookup_matrix_lines)
    value_blocks = split_blocks(value_proj)
    decay_blocks = jnp.transpose(decays.reshape(head_count, blocks, BLOCK_LEN), (1, 0, 2))
    cumulative = jnp.cumsum(decay_blocks, axis=-1)
    ending = cumulative[..., -1:]
    decay_gaps = cumulative[..., :, None] - cumulative[..., None, :]
    causal = jnp.arange(BLOCK_LEN)[:, None] >= jnp.arange(BLOCK_LEN)[None, :]
    weighting = jnp.where(causal, jnp.exp(jnp.minimum(decay_gaps, 0.0)), 0.0)
    raw_scores = jnp.einsum(
        "nhid,nhjd->nhij", query_blocks, key_blocks, preferred_element_type=jnp.float32
    )
    scores = (raw_scores * weighting).astype(jnp.bfloat16)
    intra_out = jnp.einsum(
        "nhij,nhje->nhie", scores, value_blocks, preferred_element_type=jnp.float32
    )
    decayed_keys = (
        key_blocks.astype(jnp.float32) * jnp.exp(ending - cumulative)[..., None]
    ).astype(jnp.bfloat16)
    decayed_queries = (query_blocks.astype(jnp.float32) * jnp.exp(cumulative)[..., None]).astype(
        jnp.bfloat16
    )
    block_kv = jnp.einsum(
        "nhjd,nhje->nhde", decayed_keys, value_blocks, preferred_element_type=jnp.float32
    )
    block_ends = ending[..., 0]

    def advance(state_now, step_in):
        kv_block, total = step_in
        return (state_now * jnp.exp(total)[:, None, None] + kv_block, state_now)

    start_state = jnp.zeros((head_count, KEY_DIM, VALUE_DIM), jnp.float32)
    end_state, before_local = lax.scan(advance, start_state, (block_kv, block_ends))
    device_total = jnp.sum(block_ends, axis=0)
    return (intra_out, decayed_queries, before_local, block_ends, end_state, device_total)


def combine(earlier, later):
    return (earlier[0] * jnp.exp(later[1])[:, None, None] + later[0], earlier[1] + later[1])


def carried(end_state, device_total):
    identity = (jnp.zeros_like(end_state), jnp.zeros_like(device_total))
    state_in, _ = entering((end_state, device_total), "sp", combine, identity)
    return state_in


def retention_finish(local_parts, state_in, gate_proj):
    intra_out, decayed_queries, before_local, block_ends, end_state, device_total = local_parts
    starts = jnp.cumsum(block_ends, axis=0) - block_ends
    full_states = before_local + jnp.exp(starts)[:, :, None, None] * state_in[None]
    cross = jnp.einsum(
        "nhid,nhde->nhie",
        decayed_queries,
        full_states.astype(jnp.bfloat16),
        preferred_element_type=jnp.float32,
    )
    output = intra_out + cross
    output = output * lax.rsqrt(jnp.mean(output * output, axis=-1, keepdims=True) + EPSILON)
    tok_rows = gate_proj.shape[0]
    output = jnp.transpose(output, (0, 2, 1, 3)).reshape(tok_rows, gate_proj.shape[1])
    return (output * jax.nn.silu(gate_proj.astype(jnp.float32))).astype(jnp.bfloat16)


def convolve(conv_proj, conv_kernel):
    gate_b, gate_c, conv_input = conv_proj
    tok_rows = gate_b.shape[0]
    product = gate_c.astype(jnp.float32) * conv_input.astype(jnp.float32)
    rim_rows = passed_along(product[tok_rows - (CONV_TAPS - 1) :], "sp", 1)
    padded = jnp.concatenate([rim_rows, product], axis=0)
    convolved = jnp.zeros_like(product)
    for tap_index in range(CONV_TAPS):
        convolved = convolved + conv_kernel[tap_index] * padded[tap_index : tap_index + tok_rows]
    return (gate_b.astype(jnp.float32) * convolved).astype(jnp.bfloat16)


def shards(
    tokens,
    norm_gain,
    query_weight,
    key_weight,
    value_weight,
    gate_weight,
    conv_b_weight,
    conv_c_weight,
    conv_in_weight,
    conv_kernel,
    out_ret_weight,
    out_conv_weight,
    log_decay,
):
    inputs = tokens[0].astype(jnp.float32)
    tok_rows = inputs.shape[0]
    normed = (
        inputs * lax.rsqrt(jnp.mean(inputs * inputs, axis=-1, keepdims=True) + EPSILON) * norm_gain
    ).astype(jnp.bfloat16)
    token_ordinal = (
        lax.axis_index("sp") * tok_rows + jnp.arange(tok_rows, dtype=jnp.int32)
    ).astype(jnp.float32)
    decays = log_decay[0]
    gathered = make_adder(
        normed,
        7,
        (
            lax.all_gather(query_weight, ("sp", "fs"), axis=0, tiled=True),
            lax.all_gather(key_weight, ("sp", "fs"), axis=0, tiled=True),
            lax.all_gather(value_weight, ("sp", "fs"), axis=0, tiled=True),
            lax.all_gather(gate_weight, ("sp", "fs"), axis=0, tiled=True),
            lax.all_gather(conv_b_weight, ("sp", "fs"), axis=0, tiled=True),
            lax.all_gather(conv_c_weight, ("sp", "fs"), axis=0, tiled=True),
            lax.all_gather(conv_in_weight, ("sp", "fs"), axis=0, tiled=True),
            lax.all_gather(out_ret_weight, ("sp", "fs"), axis=0, tiled=True),
            lax.all_gather(out_conv_weight, ("sp", "fs"), axis=0, tiled=True),
        ),
    )
    ret_proj = [member.astype(jnp.bfloat16) for member in gathered[:4]]
    local_parts = retention_local(ret_proj, decays, token_ordinal)
    state_in = carried(local_parts[4], local_parts[5])
    conv_proj = [member.astype(jnp.bfloat16) for member in gathered[4:7]]
    full_ret, full_conv = (gathered[7], gathered[8])
    conv_out = convolve(conv_proj, conv_kernel)
    ret_out = retention_finish(local_parts, state_in, ret_proj[3])
    partial_value = lax.dot_general(
        ret_out, full_ret, (((1,), (1,)), ((), ())), preferred_element_type=jnp.float32
    )
    mixed = lax.psum_scatter(
        (
            partial_value
            + lax.dot_general(
                conv_out, full_conv, (((1,), (1,)), ((), ())), preferred_element_type=jnp.float32
            )
        ).astype(jnp.bfloat16),
        "tp",
        scatter_dimension=0,
        tiled=True,
    )
    return mixed[None]


def solution(mesh):
    in_specs = (
        P("fs", "sp", None),
        P(),
        P(("sp", "fs"), "tp"),
        P(("sp", "fs"), "tp"),
        P(("sp", "fs"), "tp"),
        P(("sp", "fs"), "tp"),
        P(("sp", "fs"), "tp"),
        P(("sp", "fs"), "tp"),
        P(("sp", "fs"), "tp"),
        P(None, "tp"),
        P(("sp", "fs"), "tp"),
        P(("sp", "fs"), "tp"),
        P("fs", "tp", "sp"),
    )
    out_specs = P("fs", ("sp", "tp"), None)
    return jax.shard_map(shards, mesh=mesh, in_specs=in_specs, out_specs=out_specs, check_vma=False)
```

profile of v0, /device:TPU:0, one launch (start us, length us, event | category | flops | bytes accessed | tf_op | source)
XLA Modules:
  0.0 586.8 jit_solution(14236262368316451906)
XLA Ops:
  13.5 2.6 fusion.3
  20.7 13.5 %all-reduce = bf16[16]{0:T(256)(128)(2,1)S(1)} all-reduce(bf16[16]{0:T(256)(128)(2,1)S(1)} %dynamic-update-slice), channel_id=2, replica_groups=mesh['sp'=4,'fs'=4,'tp'=2] {'sp'}, use_global_device_ids=true, to_apply=%add | all-reduce | flops 16 | bytes 64
  36.7 31.3 %all-gather.12.cloned.1.call-done = bf16[2048,256]{1,0:T(8,128)(2,1)} async-done(((bf16[128,256]{1,0:T(8,128)(2,1)}), bf16[2048,256]{1,0:T(8,128)(2,1)}) %all-gather.12.cloned.1.call-update) | async-done | bytes 1048592 | tf_op jit(solution)/shard_map/all_gather | solution.py:184
  68.0 3.3 convolution_convert_fusion.6
  71.2 53.5 %all-gather.14.cloned.1.call-done = bf16[2048,256]{1,0:T(8,128)(2,1)} async-done(((bf16[128,256]{1,0:T(8,128)(2,1)}), bf16[2048,256]{1,0:T(8,128)(2,1)}) %all-gather.14.cloned.1.call-update) | async-done | bytes 1048592 | tf_op jit(solution)/shard_map/all_gather | solution.py:185
  124.7 2.6 convolution_convert_fusion.5
  129.3 57.4 %all-gather.16.cloned.1.call-done = bf16[2048,512]{1,0:T(8,128)(2,1)} async-done(((bf16[128,512]{1,0:T(8,128)(2,1)}), bf16[2048,512]{1,0:T(8,128)(2,1)}) %all-gather.16.cloned.1.call-update) | async-done | bytes 2097168 | tf_op jit(solution)/shard_map/all_gather | solution.py:186
  186.7 4.3 convolution_convert_fusion.4
  194.3 4.7 while.27
  199.0 14.9 %all-gather.1 = bf16[16,64,128]{2,1,0:T(8,128)(2,1)S(1)} all-gather(bf16[4,64,128]{2,1,0:T(8,128)(2,1)S(1)} %convert_element_type.151), channel_id=3, replica_groups=mesh['sp'=4,'fs'=4,'tp'=2] {'sp'}, dimensions={0}, use_global_device_ids=true | all-gather | bytes 327680 | tf_op jit(solution)/shard_map/all_gather | solution.py:19
  214.5 2.0 fusion.38
  216.6 3.3 multiply_reduce_fusion
  223.0 26.2 %all-gather.26.cloned.1.call-done = bf16[2048,512]{1,0:T(8,128)(2,1)} async-done(((bf16[128,512]{1,0:T(8,128)(2,1)}), bf16[2048,512]{1,0:T(8,128)(2,1)}) %all-gather.26.cloned.1.call-update) | async-done | bytes 2097168 | tf_op jit(solution)/shard_map/all_gather | solution.py:190
  249.2 5.3 convolution_convert_fusion
  254.5 56.5 %all-gather.24.cloned.1.call-done = bf16[2048,512]{1,0:T(8,128)(2,1)} async-done(((bf16[128,512]{1,0:T(8,128)(2,1)}), bf16[2048,512]{1,0:T(8,128)(2,1)}) %all-gather.24.cloned.1.call-update) | async-done | bytes 2097168 | tf_op jit(solution)/shard_map/all_gather | solution.py:189
  311.0 3.6 convert_multiply_fusion.3
  315.8 3.4 collective-permute-start
  319.1 53.7 %all-gather.18.cloned.1.call-done = bf16[2048,512]{1,0:T(8,128)(2,1)} async-done(((bf16[128,512]{1,0:T(8,128)(2,1)}), bf16[2048,512]{1,0:T(8,128)(2,1)}) %all-gather.18.cloned.1.call-update) | async-done | bytes 2097168 | tf_op jit(solution)/shard_map/all_gather | solution.py:187
  372.8 62.0 %all-gather.20.cloned.1.call-done = bf16[2048,512]{1,0:T(8,128)(2,1)} async-done(((bf16[128,512]{1,0:T(8,128)(2,1)}), bf16[2048,512]{1,0:T(8,128)(2,1)}) %all-gather.20.cloned.1.call-update) | async-done | bytes 2097168 | tf_op jit(solution)/shard_map/all_gather | solution.py:191
  434.8 9.0 %fusion.18 = f32[768,2048]{1,0:T(8,128)} fusion(bf16[2048,512]{1,0:T(8,128)(2,1)} %all-gather.20.cloned.1.call-done, f32[96,8,4,128]{3,2,1,0:T(4,128)} %bitcast.110, bf16[2048,512]{1,0:T(8,128)(2,1)} %all-gather.18.cloned.1.call-done, bf16[1,768,2048]{2,1,0:T(8,128)(2,1)S(1)} %copy-done.1, f32[2048]{0:T(1024)S(1)} %copy-done.16, f32[768]{0:T(1024)S(1)} %copy-done.10), kind=kOutput, calls=%fused_computation.43 | convolution fusion | flops 3230662656 | bytes 15215616 | tf_op jit(solution)/shard_map/dot_general | solution.py:202
  443.8 53.0 %all-gather.22.cloned.1.call-done = bf16[2048,512]{1,0:T(8,128)(2,1)} async-done(((bf16[128,512]{1,0:T(8,128)(2,1)}), bf16[2048,512]{1,0:T(8,128)(2,1)}) %all-gather.22.cloned.1.call-update) | async-done | bytes 2097168 | tf_op jit(solution)/shard_map/all_gather | solution.py:188
  496.8 62.0 %all-gather.28.cloned.1.call-done = bf16[2048,512]{1,0:T(8,128)(2,1)} async-done(((bf16[128,512]{1,0:T(8,128)(2,1)}), bf16[2048,512]{1,0:T(8,128)(2,1)}) %all-gather.28.cloned.1.call-update) | async-done | bytes 2097168 | tf_op jit(solution)/shard_map/all_gather | solution.py:192
  558.8 11.0 %add_convert_fusion = bf16[768,2048]{1,0:T(8,128)(2,1)} fusion(f32[768,2048]{1,0:T(8,128)} %fusion.18, bf16[2048,512]{1,0:T(8,128)(2,1)} %all-gather.28.cloned.1.call-done, f32[2,512]{1,0:T(2,128)S(1)} %collective-permute-done, f32[768,512]{1,0:T(8,128)} %copy-done.14, bf16[2048,512]{1,0:T(8,128)(2,1)} %all-gather.22.cloned.1.call-done, ...), kind=kOutput, calls=%fused_computation.13 | convolution fusion | flops 3234988032 | bytes 18371584 | tf_op jit(solution)/shard_map/dot_general | solution.py:208
  569.9 10.1 %reduce-scatter.2.cloned.1.call-done = bf16[384,2048]{1,0:T(8,128)(2,1)} async-done(((bf16[768,2048]{1,0:T(8,128)(2,1)}), bf16[384,2048]{1,0:T(8,128)(2,1)}) %reduce-scatter.2.cloned.1.call-update) | async-done | bytes 1572880 | tf_op jit(solution)/shard_map/reduce_scatter | solution.py:205
  (120 shorter events, 28.3 us)
Async XLA Ops:
  6.5 61.4 %all-gather.12.cloned.1.call-start = ((), (), s32[]{:S(2)}) async-start(), calls=%async_computation.1 | async-start | bytes 1114112 | tf_op jit(solution)/shard_map/all_gather | solution.py:184
  7.3 9.4 %copy-start.8 = (f32[1,4,768]{2,1,0:T(4,128)S(1)}, f32[1,4,768]{2,1,0:T(4,128)}, u32[]{:S(2)}) copy-start(f32[1,4,768]{2,1,0:T(4,128)} %param.31) | copy-start | bytes 36868
  7.3 117.4 %all-gather.14.cloned.1.call-start = ((), (), s32[]{:S(2)}) async-start(), calls=%async_computation.2 | async-start | bytes 1114112 | tf_op jit(solution)/shard_map/all_gather | solution.py:185
  8.0 178.7 %all-gather.16.cloned.1.call-start = ((), (), s32[]{:S(2)}) async-start(), calls=%async_computation.3 | async-start | bytes 2228224 | tf_op jit(solution)/shard_map/all_gather | solution.py:186
  8.8 10.2 %copy-start.18 = (u32[32]{0:T(128)S(1)}, u32[32]{0:T(128)}, u32[]{:S(2)}) copy-start(u32[32]{0:T(128)} %constant.80) | copy-start | bytes 388
  8.8 26.2 %copy-start.9 = (f32[3,512]{1,0:T(4,128)S(1)}, f32[3,512]{1,0:T(4,128)}, u32[]{:S(2)}) copy-start(f32[3,512]{1,0:T(4,128)} %param.28) | copy-start | bytes 18436
  8.8 240.4 %all-gather.26.cloned.1.call-start = ((), (), s32[]{:S(2)}) async-start(), calls=%async_computation.8 | async-start | bytes 2228224 | tf_op jit(solution)/shard_map/all_gather | solution.py:190
  9.3 301.7 %all-gather.24.cloned.1.call-start = ((), (), s32[]{:S(2)}) async-start(), calls=%async_computation.7 | async-start | bytes 2228224 | tf_op jit(solution)/shard_map/all_gather | solution.py:189
  9.9 58.0 %copy-start = (bf16[1,768,2048]{2,1,0:T(8,128)(2,1)S(1)}, bf16[1,768,2048]{2,1,0:T(8,128)(2,1)}, u32[]{:S(2)}) copy-start(bf16[1,768,2048]{2,1,0:T(8,128)(2,1)} %param.19) | copy-start | bytes 9437188
  9.9 362.9 %all-gather.18.cloned.1.call-start = ((), (), s32[]{:S(2)}) async-start(), calls=%async_computation.4 | async-start | bytes 2228224 | tf_op jit(solution)/shard_map/all_gather | solution.py:187
  10.5 424.3 %all-gather.20.cloned.1.call-start = ((), (), s32[]{:S(2)}) async-start(), calls=%async_computation.5 | async-start | bytes 2228224 | tf_op jit(solution)/shard_map/all_gather | solution.py:191
  11.3 485.5 %all-gather.22.cloned.1.call-start = ((), (), s32[]{:S(2)}) async-start(), calls=%async_computation.6 | async-start | bytes 2228224 | tf_op jit(solution)/shard_map/all_gather | solution.py:188
  12.0 546.8 %all-gather.28.cloned.1.call-start = ((), (), s32[]{:S(2)}) async-start(), calls=%async_computation.9 | async-start | bytes 2228224 | tf_op jit(solution)/shard_map/all_gather | solution.py:192
  12.8 567.2 %reduce-scatter.2.cloned.1.call-start = ((), (), s32[]{:S(2)}) async-start(), calls=%async_computation.10 | async-start | bytes 4718592 | tf_op jit(solution)/shard_map/reduce_scatter | solution.py:205
  36.7 88.0 %copy-start.10 = (f32[768]{0:T(1024)S(1)}, f32[768]{0:T(1024)}, u32[]{:S(2)}) copy-start(f32[768]{0:T(1024)} %add_rsqrt_fusion) | copy-start | bytes 9220
  127.5 59.2 %copy-start.15 = (f32[2048]{0:T(1024)S(1)}, f32[2048]{0:T(1024)}, u32[]{:S(2)}) copy-start(f32[2048]{0:T(1024)} %param.20) | copy-start | bytes 24580
  194.3 19.7 %copy-start.17 = (bf16[4,4]{1,0:T(4,128)(2,1)S(1)}, bf16[4,4]{1,0:T(4,128)(2,1)}, u32[]{:S(2)}) copy-start(bf16[4,4]{1,0:T(4,128)(2,1)} %reshape.146) | copy-start | bytes 100
  214.0 2.6 copy-start.4
  221.5 27.7 %copy-start.16 = (f32[2048]{0:T(1024)S(1)}, f32[2048]{0:T(1024)}, u32[]{:S(2)}) copy-start(f32[2048]{0:T(1024)} %param.20) | copy-start | bytes 24580
  223.0 88.0 %copy-start.1 = (bf16[1,768,2048]{2,1,0:T(8,128)(2,1)S(1)}, bf16[1,768,2048]{2,1,0:T(8,128)(2,1)}, u32[]{:S(2)}) copy-start(bf16[1,768,2048]{2,1,0:T(8,128)(2,1)} %param.19) | copy-start | bytes 9437188
  315.8 243.0 %collective-permute-start = (f32[2,512]{1,0:T(2,128)S(1)}, f32[2,512]{1,0:T(2,128)S(1)}, u32[]{:S(2)}, u32[]{:S(2)}) collective-permute-start(f32[2,512]{1,0:T(2,128)S(1)} %slice.49), channel_id=1, source_target_pairs={{0,8},{8,16},{16,24},{1,9},{9,17},{17,25},{2,10},{10,18},{18,26},{... | collective-permute-start | bytes 12296 | tf_op jit(solution)/shard_map/ppermute | solution.py:38
  434.8 124.0 %copy-start.11 = (f32[1,512]{1,0:T(1,128)S(1)}, f32[1,512]{1,0:T(1,128)}, u32[]{:S(2)}) copy-start(f32[1,512]{1,0:T(1,128)} %get-tuple-element.212) | copy-start | bytes 6148
  434.8 124.0 %copy-start.12 = (f32[1,512]{1,0:T(1,128)S(1)}, f32[1,512]{1,0:T(1,128)}, u32[]{:S(2)}) copy-start(f32[1,512]{1,0:T(1,128)} %get-tuple-element.213) | copy-start | bytes 6148
  434.8 124.0 %copy-start.13 = (f32[1,512]{1,0:T(1,128)S(1)}, f32[1,512]{1,0:T(1,128)}, u32[]{:S(2)}) copy-start(f32[1,512]{1,0:T(1,128)} %get-tuple-element.214) | copy-start | bytes 6148
  (6 other events, 14.1 us)
Sparse Core Ops, SparseCore 0:
  10.1 57.8 all-gather.11
  70.7 53.9 all-gather.13
  127.5 59.2 all-gather.15
  189.3 59.7 all-gather.25
  251.8 59.1 all-gather.23
  313.6 59.1 all-gather.17
  375.6 59.1 all-gather.19
  437.6 59.1 all-gather.21
  499.6 59.1 all-gather.27
  570.0 9.9 reduce-scatter.1
where the time goes:
time: 587 us
  waiting for transfers between devices  471 us (80%)
  matrix products  45.9 us (8%)
  blocking collectives  28.4 us (5%)
  between operations  14.5 us (2%)
  other arithmetic  14 us (2%)
  local copies, waits for them, and re-layouts  8.81 us (2%)
    all_gather x1, waiting for transfers between devices, shards(): lax.all_gather(out_conv_weight, ('sp', 'fs'), axis=0, tiled=True)  62 us
    all_gather x1, waiting for transfers between devices, shards(): lax.all_gather(out_ret_weight, ('sp', 'fs'), axis=0, tiled=True)  62 us
    all_gather x1, waiting for transfers between devices, shards(): lax.all_gather(value_weight, ('sp', 'fs'), axis=0, tiled=True)  57.4 us
    all_gather x1, waiting for transfers between devices, shards(): lax.all_gather(conv_c_weight, ('sp', 'fs'), axis=0, tiled=True)  56.5 us
    all_gather x1, waiting for transfers between devices, shards(): lax.all_gather(gate_weight, ('sp', 'fs'), axis=0, tiled=True)  53.7 us
    all_gather x1, waiting for transfers between devices, shards(): lax.all_gather(key_weight, ('sp', 'fs'), axis=0, tiled=True)  53.5 us
    all_gather x1, waiting for transfers between devices, shards(): lax.all_gather(conv_b_weight, ('sp', 'fs'), axis=0, tiled=True)  53 us
    all_gather x1, waiting for transfers between devices, shards(): lax.all_gather(query_weight, ('sp', 'fs'), axis=0, tiled=True)  31.3 us
  transfers between devices with their start and end apart: 11, of which 10 were waited for; matrix products, arithmetic and copies ran while one was open for 10% of the time, Pallas kernels for 0%

commit v1 on v0

--- a/solution.py
+++ b/solution.py
@@ -1,6 +1,8 @@
 import jax
 import jax.numpy as jnp
 from jax import lax
+from jax.experimental import pallas as pl
+from jax.experimental.pallas import tpu as pltpu
 from jax.sharding import PartitionSpec as P
 
 KEY_DIM = 64
@@ -216,6 +218,438 @@
     return mixed[None]
 
 
+MESH_IDS = pl.DeviceIdType.MESH
+
+
+def remote(source, target, sent, landed, device):
+    return pltpu.make_async_remote_copy(
+        src_ref=source,
+        dst_ref=target,
+        send_sem=sent,
+        recv_sem=landed,
+        device_id=device,
+        device_id_type=MESH_IDS,
+    )
+
+
+def greet(peers):
+    barrier = pltpu.get_barrier_semaphore()
+    for peer in peers:
+        pl.semaphore_signal(barrier, inc=1, device_id=peer, device_id_type=MESH_IDS)
+    pl.semaphore_wait(barrier, len(peers))
+
+
+def plane_partners(f):
+    x, y = f % 2, f // 2
+    return y * 2 + (1 - x), (1 - y) * 2 + x, 3 - f
+
+
+def gather_kernel(
+    n_sp,
+    half_ref,
+    weight_ref,
+    decay_ref,
+    normed_ref,
+    full_ref,
+    decays_ref,
+    norm_sent,
+    norm_landed,
+    side_sent,
+    side_landed,
+    relay_sent,
+    weight_sent,
+    weight_landed,
+    up_sent,
+    down_sent,
+    line_landed,
+    decay_sent,
+    decay_landed,
+    local_sem,
+):
+    s, f, t = lax.axis_index("sp"), lax.axis_index("fs"), lax.axis_index("tp")
+    xn, yn, dn = plane_partners(f)
+    half = half_ref.shape[0]
+    chunk = half // 2
+    rows = weight_ref.shape[1]
+    n_fs = weight_ref.shape[0]
+    other = {"tp": 1 - t}
+    peers = [{"fs": xn}, {"fs": yn}, {"fs": dn}, other]
+    peers += [{"sp": (s + d) % n_sp} for d in range(1, n_sp)]
+    greet(peers)
+
+    def spot(owner, core, piece):
+        return normed_ref.at[owner, pl.ds(core * half + piece * chunk, chunk), :]
+
+    def own(piece):
+        return half_ref.at[pl.ds(piece * chunk, chunk), :]
+
+    def block(b, g):
+        return full_ref.at[pl.ds((b * n_fs + g) * rows, rows), :]
+
+    waits = []
+    locals_ = []
+
+    def start(copy):
+        copy.start()
+        waits.append(copy)
+
+    order = (xn, yn, dn)
+    for i, p in enumerate(order):
+        start(remote(weight_ref.at[p], block(s, f), weight_sent.at[i], weight_landed.at[f], {"fs": p}))
+    for i, p in enumerate(order):
+        start(remote(decay_ref.at[p], decays_ref.at[f], decay_sent.at[i], decay_landed.at[f], {"fs": p}))
+    start(remote(own(0), spot(f, t, 0), norm_sent.at[0], norm_landed.at[f, 0], {"fs": xn}))
+    start(remote(own(1), spot(f, t, 1), norm_sent.at[1], norm_landed.at[f, 1], {"fs": yn}))
+    start(remote(own(1), spot(f, t, 1), norm_sent.at[2], norm_landed.at[f, 1], {"fs": xn}))
+    start(remote(own(0), spot(f, t, 0), norm_sent.at[3], norm_landed.at[f, 0], {"fs": yn}))
+
+    def line_copy(source, b, g, way):
+        sent = up_sent if way == 1 else down_sent
+        return remote(source, block(b, g), sent.at[b, g], line_landed.at[b, g], {"sp": s + way})
+
+    def send_line(source, b, g):
+        @pl.when(s < n_sp - 1)
+        def _():
+            line_copy(source, b, g, 1).start()
+
+        @pl.when(s > 0)
+        def _():
+            line_copy(source, b, g, -1).start()
+
+    send_line(weight_ref.at[f], s, f)
+    for piece in range(2):
+        start(remote(own(piece), spot(f, t, piece), side_sent.at[f, piece], side_landed.at[f, piece], other))
+    for i, (a, b) in enumerate(
+        (
+            (own(0), spot(f, t, 0)),
+            (own(1), spot(f, t, 1)),
+            (weight_ref.at[f], block(s, f)),
+            (decay_ref.at[f], decays_ref.at[f]),
+        )
+    ):
+        copy = pltpu.make_async_copy(a, b, local_sem.at[i])
+        copy.start()
+        locals_.append(copy)
+
+    for p in order:
+        remote(weight_ref.at[p], block(s, p), weight_sent.at[0], weight_landed.at[p], {"fs": p}).wait_recv()
+        send_line(block(s, p), s, p)
+
+    def arrived(owner, piece):
+        view = spot(owner, t, piece)
+        remote(view, view, norm_sent.at[0], norm_landed.at[owner, piece], {"fs": owner}).wait_recv()
+        start(remote(view, view, side_sent.at[owner, piece], side_landed.at[owner, piece], other))
+
+    def line_step(d):
+        for g in (f,) + order:
+
+            @pl.when(s - d >= 0)
+            def _():
+                line_copy(block(s - d, g), s - d, g, 1).wait_recv()
+
+                @pl.when(s < n_sp - 1)
+                def _():
+                    line_copy(block(s - d, g), s - d, g, 1).start()
+
+            @pl.when(s + d <= n_sp - 1)
+            def _():
+                line_copy(block(s + d, g), s + d, g, -1).wait_recv()
+
+                @pl.when(s > 0)
+                def _():
+                    line_copy(block(s + d, g), s + d, g, -1).start()
+
+    arrived(xn, 0)
+    start(remote(spot(xn, t, 0), spot(xn, t, 0), relay_sent.at[0], norm_landed.at[xn, 0], {"fs": yn}))
+    arrived(yn, 1)
+    start(remote(spot(yn, t, 1), spot(yn, t, 1), relay_sent.at[1], norm_landed.at[yn, 1], {"fs": xn}))
+    line_step(1)
+    arrived(xn, 1)
+    arrived(yn, 0)
+    for d in range(2, n_sp - 1):
+        line_step(d)
+    arrived(dn, 0)
+    arrived(dn, 1)
+    if n_sp > 2:
+        line_step(n_sp - 1)
+    for p in order:
+        remote(decay_ref.at[p], decays_ref.at[p], decay_sent.at[0], decay_landed.at[p], {"fs": p}).wait_recv()
+    for owner in range(n_fs):
+        for piece in range(2):
+            view = spot(owner, 1 - t, piece)
+            remote(view, view, side_sent.at[0, 0], side_landed.at[owner, piece], other).wait_recv()
+    for copy in waits:
+        copy.wait_send()
+    for copy in locals_:
+        copy.wait()
+    for b in range(n_sp):
+        for g in range(n_fs):
+
+            @pl.when((s < n_sp - 1) & (b <= s))
+            def _():
+                line_copy(block(b, g), b, g, 1).wait_send()
+
+            @pl.when((s > 0) & (b >= s))
+            def _():
+                line_copy(block(b, g), b, g, -1).wait_send()
+
+
+def gather_all(n_sp, half, pieces, decays):
+    n_fs, rows, width = pieces.shape
+    any_space = pl.BlockSpec(memory_space=pl.ANY)
+    vmem = pl.BlockSpec(memory_space=pltpu.VMEM)
+    dma = pltpu.SemaphoreType.DMA
+    return pl.pallas_call(
+        lambda *refs: gather_kernel(n_sp, *refs),
+        out_shape=(
+            jax.ShapeDtypeStruct((n_fs, 2 * half.shape[0], half.shape[1]), jnp.bfloat16),
+            jax.ShapeDtypeStruct((n_sp * n_fs * rows, width), jnp.bfloat16),
+            jax.ShapeDtypeStruct(decays.shape, jnp.float32),
+        ),
+        in_specs=[vmem] * 3,
+        out_specs=(any_space, any_space, vmem),
+        scratch_shapes=[
+            dma((4,)),
+            dma((n_fs, 2)),
+            dma((n_fs, 2)),
+            dma((n_fs, 2)),
+            dma((2,)),
+            dma((3,)),
+            dma((n_fs,)),
+            dma((n_sp, n_fs)),
+            dma((n_sp, n_fs)),
+            dma((n_sp, n_fs)),
+            dma((3,)),
+            dma((n_fs,)),
+            dma((4,)),
+        ],
+        compiler_params=pltpu.CompilerParams(collective_id=0, has_side_effects=True),
+        cost_estimate=pl.CostEstimate(flops=0, bytes_accessed=200_000_000, transcendentals=0),
+        name="gather_all",
+    )(half, pieces, decays)
+
+
+def swap_kernel(
+    mixed_ref, weight_ref, same_ref, cross_ref, far_ref, sent, same_landed, cross_landed, weight_sems, local_sem
+):
+    f, t = lax.axis_index("fs"), lax.axis_index("tp")
+    half = same_ref.shape[1]
+    order = plane_partners(f)
+    peers = [{"fs": p, "tp": q} for p in order for q in (t, 1 - t)] + [{"tp": 1 - t}]
+    greet(peers)
+
+    def mine(p, core):
+        return mixed_ref.at[p, pl.ds(core * half, half), :]
+
+    copies = []
+    for i, p in enumerate((order[2], order[0], order[1])):
+        copies.append(
+            remote(mine(p, t), same_ref.at[f], sent.at[2 * i], same_landed.at[f], {"fs": p})
+        )
+        copies.append(
+            remote(
+                mine(p, 1 - t),
+                cross_ref.at[f],
+                sent.at[2 * i + 1],
+                cross_landed.at[f],
+                {"fs": p, "tp": 1 - t},
+            )
+        )
+    copies.append(remote(mine(f, 1 - t), cross_ref.at[f], sent.at[6], cross_landed.at[f], {"tp": 1 - t}))
+    for copy in copies:
+        copy.start()
+    weight = remote(weight_ref, far_ref, weight_sems.at[0], weight_sems.at[1], {"tp": 1 - t})
+    weight.start()
+    local = pltpu.make_async_copy(mine(f, t), same_ref.at[f], local_sem)
+    local.start()
+    for p in order:
+        remote(same_ref.at[p], same_ref.at[p], sent.at[0], same_landed.at[p], {"fs": p}).wait_recv()
+    for p in order + (f,):
+        remote(cross_ref.at[p], cross_ref.at[p], sent.at[0], cross_landed.at[p], {"tp": 1 - t}).wait_recv()
+    for copy in copies:
+        copy.wait_send()
+    local.wait()
+    weight.wait()
+
+
+def swap(mixed, weight):
+    n_fs, rows, width = mixed.shape
+    any_space = pl.BlockSpec(memory_space=pl.ANY)
+    vmem = pl.BlockSpec(memory_space=pltpu.VMEM)
+    dma = pltpu.SemaphoreType.DMA
+    piece = jax.ShapeDtypeStruct((n_fs, rows // 2, width), jnp.bfloat16)
+    return pl.pallas_call(
+        swap_kernel,
+        out_shape=(piece, piece, jax.ShapeDtypeStruct(weight.shape, weight.dtype)),
+        in_specs=[vmem, any_space],
+        out_specs=(vmem, vmem, any_space),
+        scratch_shapes=[dma((7,)), dma((n_fs,)), dma((n_fs,)), dma((2,)), dma],
+        compiler_params=pltpu.CompilerParams(collective_id=1, has_side_effects=True),
+        cost_estimate=pl.CostEstimate(flops=0, bytes_accessed=60_000_000, transcendentals=0),
+        name="swap",
+    )(mixed, weight)
+
+
+def rotate_flat(values, cosine, sine):
+    half_dim = values.shape[-1] // 2
+    first = values[..., :half_dim].astype(jnp.float32)
+    second = values[..., half_dim:].astype(jnp.float32)
+    return jnp.concatenate([first * cosine - second * sine, first * sine + second * cosine], axis=-1)
+
+
+def fast_shards(
+    tokens,
+    norm_gain,
+    query_weight,
+    key_weight,
+    value_weight,
+    gate_weight,
+    conv_b_weight,
+    conv_c_weight,
+    conv_in_weight,
+    conv_kernel,
+    out_ret_weight,
+    out_conv_weight,
+    log_decay,
+):
+    n_sp, n_fs = lax.axis_size("sp"), lax.axis_size("fs")
+    s, f, t = lax.axis_index("sp"), lax.axis_index("fs"), lax.axis_index("tp")
+    tok_rows, model = tokens.shape[1:]
+    half = tok_rows // 2
+    blocks = tok_rows // BLOCK_LEN
+    rows = query_weight.shape[0]
+    inputs = lax.dynamic_slice_in_dim(tokens[0], t * half, half).astype(jnp.float32)
+    normed = (
+        inputs * lax.rsqrt(jnp.mean(inputs * inputs, axis=-1, keepdims=True) + EPSILON) * norm_gain
+    ).astype(jnp.bfloat16)
+    pieces = jnp.concatenate(
+        [
+            jnp.transpose(w.reshape(rows, n_fs, w.shape[1] // n_fs), (1, 0, 2))
+            for w in (
+                query_weight,
+                key_weight,
+                value_weight,
+                gate_weight,
+                conv_b_weight,
+                conv_c_weight,
+                conv_in_weight,
+            )
+        ],
+        axis=-1,
+    )
+    own_out = jnp.concatenate([out_ret_weight, out_conv_weight], axis=-1)
+    out_weight = lax.all_gather(own_out, ("sp", "fs"), axis=0, tiled=True)
+    everyone, weights, decays = gather_all(
+        n_sp, normed, pieces, log_decay[0].reshape(n_fs, blocks, BLOCK_LEN)
+    )
+    proj = jnp.dot(
+        everyone.reshape(n_fs * tok_rows, model), weights, preferred_element_type=jnp.float32
+    ).astype(jnp.bfloat16)
+    proj = proj.reshape(n_fs, tok_rows, weights.shape[1])
+    cuts = (KEY_DIM, 2 * KEY_DIM)
+    q_raw, k_raw, wide = proj[..., : cuts[0]], proj[..., cuts[0] : cuts[1]], proj[..., cuts[1] :]
+    values, ret_gate, gate_b, gate_c, conv_in = jnp.split(wide, 5, axis=-1)
+
+    ordinal = (s * tok_rows + jnp.arange(tok_rows, dtype=jnp.int32)).astype(jnp.float32)
+    frequency = 1.0 / ROPE_BASE ** jnp.linspace(0.0, 1.0, KEY_DIM // 2, dtype=jnp.float32)
+    angles = ordinal[:, None] * frequency[None, :]
+    cosine, sine = jnp.cos(angles), jnp.sin(angles)
+    queries = rotate_flat(q_raw, cosine, sine).astype(jnp.bfloat16)
+    keys = (rotate_flat(k_raw, cosine, sine) * KEY_DIM ** (-0.5)).astype(jnp.bfloat16)
+
+    def cut(array):
+        return array.reshape(n_fs, blocks, BLOCK_LEN, array.shape[-1])
+
+    queries, keys, value_blocks = cut(queries), cut(keys), cut(values)
+    cumulative = jnp.cumsum(decays, axis=-1)
+    ending = cumulative[..., -1:]
+    gaps = cumulative[..., :, None] - cumulative[..., None, :]
+    causal = jnp.arange(BLOCK_LEN)[:, None] >= jnp.arange(BLOCK_LEN)[None, :]
+    weighting = jnp.where(causal, jnp.exp(jnp.minimum(gaps, 0.0)), 0.0)
+    decayed_keys = (keys.astype(jnp.float32) * jnp.exp(ending - cumulative)[..., None]).astype(
+        jnp.bfloat16
+    )
+    block_kv = jnp.einsum(
+        "bnjd,bnje->bnde", decayed_keys, value_blocks, preferred_element_type=jnp.float32
+    )
+    state = jnp.zeros_like(block_kv[:, 0])
+    start = jnp.zeros_like(ending[:, 0])
+    before, starts = [], []
+    for n in range(blocks):
+        before.append(state)
+        starts.append(start)
+        state = state * jnp.exp(ending[:, n])[..., None] + block_kv[:, n]
+        start = start + ending[:, n]
+    product = gate_c.astype(jnp.float32) * conv_in.astype(jnp.float32)
+    halo = CONV_TAPS - 1
+    packed = jnp.concatenate(
+        [
+            state,
+            product[:, tok_rows - halo :],
+            jnp.broadcast_to(start[..., None], (n_fs, 8 - halo, state.shape[-1])),
+        ],
+        axis=1,
+    )
+    shared = lax.all_gather(packed, "sp")
+    state_in = jnp.zeros_like(state)
+    rim = jnp.zeros_like(product[:, :halo])
+    for k in range(n_sp - 1):
+        part, total = shared[k, :, :KEY_DIM], shared[k, :, KEY_DIM + halo :][:, :1, :1]
+        state_in = jnp.where(k < s, state_in * jnp.exp(total) + part, state_in)
+        rim = jnp.where(k == s - 1, shared[k, :, KEY_DIM : KEY_DIM + halo], rim)
+
+    raw = jnp.einsum("bnid,bnjd->bnij", queries, keys, preferred_element_type=jnp.float32)
+    scores = (raw * weighting).astype(jnp.bfloat16)
+    intra = jnp.einsum("bnij,bnje->bnie", scores, value_blocks, preferred_element_type=jnp.float32)
+    decayed_queries = (queries.astype(jnp.float32) * jnp.exp(cumulative)[..., None]).astype(
+        jnp.bfloat16
+    )
+    full_states = (
+        jnp.stack(before, axis=1) + jnp.exp(jnp.stack(starts, axis=1))[..., None] * state_in[:, None]
+    )
+    cross = jnp.einsum(
+        "bnid,bnde->bnie",
+        decayed_queries,
+        full_states.astype(jnp.bfloat16),
+        preferred_element_type=jnp.float32,
+    )
+    output = intra + cross
+    output = output * lax.rsqrt(jnp.mean(output * output, axis=-1, keepdims=True) + EPSILON)
+    output = output.reshape(n_fs, tok_rows, values.shape[-1])
+    ret_out = (output * jax.nn.silu(ret_gate.astype(jnp.float32))).astype(jnp.bfloat16)
+
+    padded = jnp.concatenate([rim, product], axis=1)
+    width = product.shape[-1]
+    taps = lax.dynamic_slice_in_dim(conv_kernel, f * width, width, axis=1)
+    convolved = sum(taps[k] * padded[:, k : k + tok_rows] for k in range(CONV_TAPS))
+    conv_out = (gate_b.astype(jnp.float32) * convolved).astype(jnp.bfloat16)
+
+    same, cross_core, far_weight = swap(jnp.concatenate([ret_out, conv_out], axis=-1), out_weight)
+
+    def spread(piece):
+        parts = piece.reshape(n_fs, half, 2, width)
+        return jnp.transpose(parts, (1, 2, 0, 3)).reshape(half, 2 * n_fs * width)
+
+    def project(piece, weight):
+        return lax.dot_general(
+            spread(piece), weight, (((1,), (1,)), ((), ())), preferred_element_type=jnp.float32
+        )
+
+    mixed = project(same, out_weight) + project(cross_core, far_weight)
+    return mixed.astype(jnp.bfloat16)[None]
+
+
+def select(mesh):
+    def chosen(*arrays):
+        heads, conv_width = arrays[12].shape[1], arrays[9].shape[1]
+        n_sp, n_fs, n_tp = (mesh.shape[name] for name in ("sp", "fs", "tp"))
+        fits = n_fs == 4 and n_tp == 2 and n_sp > 1 and heads == n_fs
+        fits = fits and conv_width == n_fs * VALUE_DIM and arrays[0].shape[1] % (2 * BLOCK_LEN) == 0
+        return (fast_shards if fits else shards)(*arrays)
+
+    return chosen
+
+
 def solution(mesh):
     in_specs = (
         P("fs", "sp", None),
@@ -233,4 +667,4 @@
         P("fs", "tp", "sp"),
     )
     out_specs = P("fs", ("sp", "tp"), None)
-    return jax.shard_map(shards, mesh=mesh, in_specs=in_specs, out_specs=out_specs, check_vma=False)
+    return jax.shard_map(select(mesh), mesh=mesh, in_specs=in_specs, out_specs=out_specs, check_vma=False)

time: 587 us -> 230 us (0.39)
  waiting for transfers between devices: 471 us -> 0.02 us
  Pallas kernels: 0 us -> 129 us
  matrix products: 45.9 us -> 29.9 us
  other arithmetic: 14 us -> 25.9 us
  blocking collectives: 28.4 us -> 16.5 us
    all_gather x9 -> x1, waiting for transfers between devices: 455 us -> 0.01 us  [fast_shards(): out_weight = lax.all_gather(own_out, ('sp', 'fs'), axis=0, tiled=True)]
    pallas_call x0 -> x2, Pallas kernels: none -> 129 us  [the longest x1 106 us: gather_all(): pl.pallas_call(lambda *refs: gather_kernel(n_sp, *refs), out_shape=(jax.S...]
    dot_general x10 -> x6, matrix products: 45.9 us -> 29.9 us  [the longest x1 15.3 us: fast_shards(): jnp.dot(everyone.reshape(n_fs * tok_rows, model), weights, preferred_elem...]
    unnamed x1 -> x0, blocking collectives: 13.5 us -> none
    reduce_scatter x1 -> x0, waiting for transfers between devices: 10.1 us -> none  [shards(): lax.psum_scatter((partial_value + lax.dot_general(conv_out, full_conv, ((...]
  transfers between devices with their start and end apart: 11 -> 1, of which waited for: 10 -> 0; matrix products, arithmetic and copies ran while one was open for 10% -> 25% of each run, Pallas kernels for 0% -> 46%
where the time goes in v1:
time: 230 us
  Pallas kernels  129 us (56%)
  matrix products  29.9 us (13%)
  other arithmetic  25.9 us (11%)
  blocking collectives  16.5 us (7%)
  local copies, waits for them, and re-layouts  14.6 us (6%)
  between operations  14 us (6%)
    pallas_call x1, Pallas kernels, gather_all(): pl.pallas_call(lambda *refs: gather_kernel(n_sp, *refs), out_shape=(jax.S...  106 us
    pallas_call x1, Pallas kernels, swap(): pl.pallas_call(swap_kernel, out_shape=(piece, piece, jax.ShapeDtypeStruct...  22.9 us
    all_gather x1, blocking collectives, fast_shards(): shared = lax.all_gather(packed, 'sp')  16.5 us
    dot_general x1, matrix products, fast_shards(): jnp.dot(everyone.reshape(n_fs * tok_rows, model), weights, preferred_elem...  15.3 us
    dot_general x2, matrix products, project(): lax.dot_general(spread(piece), weight, (((1,), (1,)), ((), ())), preferre...  7.3 us
    another operation x1, other arithmetic  5.4 us
  transfers between devices with their start and end apart: 1, of which 0 were waited for; matrix products, arithmetic and copies ran while one was open for 25% of the time, Pallas kernels for 46%

profile of v1, /device:TPU:0, one launch (start us, length us, event | category | flops | bytes accessed | tf_op | source)
XLA Modules:
  0.0 229.7 jit_solution(6045007397258816238)
XLA Ops:
  6.5 1.7 pad_maximum_fusion.3
  8.3 1.9 fusion
  12.8 3.0 %fusion.2.refs_0_ = bf16[384,2048]{1,0:T(8,128)(2,1)} fusion(f32[2048]{0:T(1024)S(1)} %copy-done.18, f32[384]{0:T(512)S(1)} %add_rsqrt_fusion.1, bf16[1,768,2048]{2,1,0:T(8,128)(2,1)} %param.13, s32[]{:T(128)S(6)} %select_n.67), kind=kLoop, calls=%fused_computation.5 | loop fusion | flops 3145728 | bytes 3155460 | tf_op jit(solution)/shard_map/convert_element_type | solution.py:524
  15.8 1.1 concatenate.46.refs_1_
  16.9 105.8 %gather_all.1 = (bf16[4,768,2048]{2,1,0:T(8,128)(2,1)}, bf16[2048,768]{1,0:T(8,128)(2,1)}, f32[4,6,128]{2,1,0:T(8,128)}) custom-call(bf16[384,2048]{1,0:T(8,128)(2,1)} %fusion.2.refs_0_, bf16[4,128,768]{2,1,0:T(8,128)(2,1)} %concatenate.46.refs_1_, f32[4,6,128]{2,1,0:T(8,128)} %reshape_squeeze.3.refs_2_), custom_call_target="tpu_custom_call" | custom-call | bytes 200000000 | tf_op jit(solution)/shard_map/gather_all/pallas_call | solution.py:402
  122.7 15.3 %convolution_convert_fusion = bf16[3072,768]{1,0:T(8,128)(2,1)} fusion(bf16[3072,2048]{1,0:T(8,128)(2,1)} %bitcast.184, bf16[2048,768]{1,0:T(8,128)(2,1)} %get-tuple-element.12), kind=kOutput, calls=%fused_computation | convolution fusion | flops 9666035712 | bytes 20447232 | tf_op jit(solution)/shard_map/dot_general | solution.py:545
  138.0 1.1 reduce_window_sum.11
  140.0 2.1 split.20
  142.2 1.4 multiply_cosine_fusion
  143.7 5.4 %fusion.11 = (bf16[4,768,32]{2,1,0:T(8,128)(2,1)}, bf16[4,768,32]{2,1,0:T(8,128)(2,1)}, f32[4,768,32]{2,1,0:T(8,128)S(1)}, f32[4,768,32]{2,1,0:T(8,128)S(1)}) fusion(f32[768,32]{1,0:T(8,128)S(1)} %get-tuple-element.47, f32[768,32]{1,0:T(8,128)S(1)} %get-tuple-element.46, bf16[4,768,768]{2,1,0:T(8,128)(2,1)} %bitcast.151), kind=kLoop, calls=%fused_computation.27 | loop fusion | flops 1769472 | bytes 2162688 | tf_op jit(solution)/shard_map/convert.4
  149.5 1.2 copy.67
  150.7 1.7 convert_multiply_fusion.11
  153.3 1.0 copy.65
  156.7 1.4 fusion.28
  158.3 16.5 %all-gather = f32[16,72,128]{2,1,0:T(8,128)S(1)} all-gather(f32[4,72,128]{2,1,0:T(8,128)S(1)} %pad_maximum_fusion.7), channel_id=2, replica_groups=mesh['sp'=4,'fs'=4,'tp'=2] {'sp'}, dimensions={0}, use_global_device_ids=true | all-gather | bytes 737280 | tf_op jit(solution)/shard_map/all_gather | solution.py:593
  176.3 1.6 fusion.27
  178.0 4.4 %multiply_reduce_fusion = (f32[4,6,128]{2,1,0:T(8,128)}, f32[4,6,128,128]{3,2,1,0:T(8,128)}) fusion(f32[4,6,128,128]{3,2,1,0:T(8,128)} %fusion.27, bf16[4,6,128,128]{3,2,1,0:T(8,128)(2,1)S(1)} %bitcast.159, f32[4,6,128]{2,1,0:T(8,128)} %copy-done.8, pred[128,128]{1,0:T(8,128)(4,1)} %iota_compare_fusion, bf16[4,6,128,32]{2,3,1,0:T(8,128)(2,1)S(1)} %copy-done.7, ...), kind=kOutput, calls=%fused_computation.39 | convolution fusion | flops 155513856 | bytes 5152768 | tf_op jit(solution)/shard_map/bnij,bnje->bnie/dot_general | solution.py:603
  183.1 1.9 broadcast_multiply_fusion
  185.0 2.5 %fusion.21 = (bf16[4,768,128]{2,1,0:T(8,128)(2,1)S(1)}, bf16[4,768,128]{2,1,0:T(8,128)(2,1)S(1)}) fusion(f32[4,6,128,128]{3,2,1,0:T(8,128)S(1)} %broadcast_multiply_fusion, bf16[4,768,768]{2,1,0:T(8,128)(2,1)} %bitcast.153, f32[4,768,128]{2,1,0:T(8,128)S(1)} %convert_multiply_fusion.11, f32[128]{0:T(128)S(1)} %copy-done.27, f32[4,2,128]{2,1,0:T(2,128)S(1)} %fusion.51, ...), kind=kLoop, calls=%fused_computation.42 | loop fusion | flops 6684672 | bytes 6297088 | tf_op jit(solution)/shard_map/convert_element_type | solution.py:619
  187.5 1.3 pad_maximum_fusion.1.mixed_ref
  188.9 22.9 %swap.1 = (bf16[4,384,256]{2,1,0:T(8,128)(2,1)}, bf16[4,384,256]{2,1,0:T(8,128)(2,1)}, bf16[2048,1024]{1,0:T(8,128)(2,1)}) custom-call(bf16[4,768,256]{2,1,0:T(8,128)(2,1)} %pad_maximum_fusion.1.mixed_ref, bf16[2048,1024]{1,0:T(8,128)(2,1)} %all-gather.3.cloned.1.call-done.weight_ref), custom_call_target="tpu_custom_call" | custom-call | bytes 60000000 | tf_op jit(solution)/shard_map/swap/pallas_call | solution.py:481
  211.8 2.1 reshape.320
  215.6 4.2 %fusion.72 = f32[384,2048]{1,0:T(8,128)S(1)} fusion(bf16[384,1024]{0,1:T(8,128)(2,1)S(1)} %bitcast.163, bf16[2048,1024]{1,0:T(8,128)(2,1)} %all-gather.3.cloned.1.call-done.weight_ref), kind=kOutput, calls=%fused_computation.145 | convolution fusion | flops 1610612736 | bytes 8126464 | tf_op jit(solution)/shard_map/dot_general | solution.py:634
  219.8 3.1 %fusion.3 = bf16[1,384,2048]{2,1,0:T(8,128)(2,1)} fusion(f32[384,2048]{1,0:T(8,128)S(1)} %fusion.72, bf16[384,1024]{0,1:T(8,128)(2,1)S(1)} %bitcast.164, bf16[2048,1024]{1,0:T(8,128)(2,1)S(1)} %copy-done.30), kind=kOutput, calls=%fused_computation.7 | convolution fusion | flops 1612185600 | bytes 9699328 | tf_op jit(solution)/shard_map/dot_general | solution.py:634
  (115 shorter events, 11.1 us)
Async XLA Ops:
  6.5 147.8 %copy-start = (f32[3,512]{1,0:T(4,128)S(1)}, f32[3,512]{1,0:T(4,128)}, u32[]{:S(2)}) copy-start(f32[3,512]{1,0:T(4,128)} %param.22) | copy-start | bytes 18436
  6.5 3.7 %copy-start.9 = (bf16[128,512]{1,0:T(8,128)(2,1)S(1)}, bf16[128,512]{1,0:T(8,128)(2,1)}, u32[]{:S(2)}) copy-start(bf16[128,512]{1,0:T(8,128)(2,1)} %param.19) | copy-start | bytes 393220
  6.5 4.0 %copy-start.10 = (bf16[128,512]{1,0:T(8,128)(2,1)S(1)}, bf16[128,512]{1,0:T(8,128)(2,1)}, u32[]{:S(2)}) copy-start(bf16[128,512]{1,0:T(8,128)(2,1)} %param.20) | copy-start | bytes 393220
  6.5 182.3 %all-gather.3.cloned.1.call-start = ((), (), s32[]{:S(2)}) async-start(), calls=%async_computation | async-start | bytes 4456448 | tf_op jit(solution)/shard_map/all_gather | solution.py:541
  8.3 2.5 %copy-start.11 = (bf16[128,512]{1,0:T(8,128)(2,1)S(1)}, bf16[128,512]{1,0:T(8,128)(2,1)}, u32[]{:S(2)}) copy-start(bf16[128,512]{1,0:T(8,128)(2,1)} %param.21) | copy-start | bytes 393220
  8.3 2.8 %copy-start.12 = (bf16[128,512]{1,0:T(8,128)(2,1)S(1)}, bf16[128,512]{1,0:T(8,128)(2,1)}, u32[]{:S(2)}) copy-start(bf16[128,512]{1,0:T(8,128)(2,1)} %param.17) | copy-start | bytes 393220
  8.3 3.0 %copy-start.13 = (bf16[128,512]{1,0:T(8,128)(2,1)S(1)}, bf16[128,512]{1,0:T(8,128)(2,1)}, u32[]{:S(2)}) copy-start(bf16[128,512]{1,0:T(8,128)(2,1)} %param.18) | copy-start | bytes 393220
  10.4 2.4 %copy-start.18 = (f32[2048]{0:T(1024)S(1)}, f32[2048]{0:T(1024)}, u32[]{:S(2)}) copy-start(f32[2048]{0:T(1024)} %param.14) | copy-start | bytes 24580
  122.7 15.3 %copy-start.16 = (f32[4,6,128]{2,1,0:T(8,128)S(1)}, f32[4,6,128]{2,1,0:T(8,128)}, u32[]{:S(2)}) copy-start(f32[4,6,128]{2,1,0:T(8,128)} %get-tuple-element.13) | copy-start | bytes 36868
  139.1 4.5 %copy-start.8 = (f32[4,6,128]{2,1,0:T(8,128)}, f32[4,6,128]{2,1,0:T(8,128)S(1)}, u32[]{:S(2)}) copy-start(f32[4,6,128]{2,1,0:T(8,128)S(1)} %reduce_window_sum.11) | copy-start | bytes 36868
  150.7 2.6 %copy-start.1 = (bf16[4,768,32]{2,1,0:T(8,128)(2,1)S(1)}, bf16[4,768,32]{2,1,0:T(8,128)(2,1)}, u32[]{:S(2)}) copy-start(bf16[4,768,32]{2,1,0:T(8,128)(2,1)} %get-tuple-element.36) | copy-start | bytes 589828
  153.3 3.3 %copy-start.3 = (bf16[4,768,128]{2,1,0:T(8,128)(2,1)S(1)}, bf16[4,768,128]{2,1,0:T(8,128)(2,1)}, u32[]{:S(2)}) copy-start(bf16[4,768,128]{2,1,0:T(8,128)(2,1)} %split.20) | copy-start | bytes 2359300
  154.3 3.7 %copy-start.19 = (f32[4]{0:T(128)S(1)}, f32[4]{0:T(128)}, u32[]{:S(2)}) copy-start(f32[4]{0:T(128)} %get-tuple-element.23) | copy-start | bytes 52
  154.3 3.7 %copy-start.20 = (f32[4]{0:T(128)S(1)}, f32[4]{0:T(128)}, u32[]{:S(2)}) copy-start(f32[4]{0:T(128)} %get-tuple-element.25) | copy-start | bytes 52
  154.3 3.7 %copy-start.21 = (f32[4]{0:T(128)S(1)}, f32[4]{0:T(128)}, u32[]{:S(2)}) copy-start(f32[4]{0:T(128)} %get-tuple-element.21) | copy-start | bytes 52
  154.3 3.7 %copy-start.23 = (f32[4]{0:T(128)S(1)}, f32[4]{0:T(128)}, u32[]{:S(2)}) copy-start(f32[4]{0:T(128)} %get-tuple-element.22) | copy-start | bytes 52
  154.3 3.7 %copy-start.24 = (f32[4]{0:T(128)S(1)}, f32[4]{0:T(128)}, u32[]{:S(2)}) copy-start(f32[4]{0:T(128)} %get-tuple-element.24) | copy-start | bytes 52
  154.3 3.7 %copy-start.25 = (f32[4]{0:T(128)S(1)}, f32[4]{0:T(128)}, u32[]{:S(2)}) copy-start(f32[4]{0:T(128)} %get-tuple-element.26) | copy-start | bytes 52
  158.3 17.9 %copy-start.22 = (f32[4]{0:T(128)S(1)}, f32[4]{0:T(128)}, u32[]{:S(2)}) copy-start(f32[4]{0:T(128)} %get-tuple-element.21) | copy-start | bytes 52
  183.1 1.9 copy-start.26
  183.1 1.9 copy-start.27
  183.1 1.9 copy-start.28
  211.8 2.8 %copy-start.5 = (bf16[4,384,256]{2,1,0:T(8,128)(2,1)S(1)}, bf16[4,384,256]{2,1,0:T(8,128)(2,1)}, u32[]{:S(2)}) copy-start(bf16[4,384,256]{2,1,0:T(8,128)(2,1)} %get-tuple-element.15) | copy-start | bytes 2359300
  215.5 4.2 %copy-start.30 = (bf16[2048,1024]{1,0:T(8,128)(2,1)S(1)}, bf16[2048,1024]{1,0:T(8,128)(2,1)}, u32[]{:S(2)}) copy-start(bf16[2048,1024]{1,0:T(8,128)(2,1)} %get-tuple-element.16) | copy-start | bytes 12582916
  (8 other events, 12.8 us)
Sparse Core Ops, SparseCore 0:
  10.1 108.5 all-gather.2

commit v2 on v1

--- a/solution.py
+++ b/solution.py
@@ -249,9 +249,12 @@
     half_ref,
     weight_ref,
     decay_ref,
+    out_ref,
+    proj_ref,
+    decays_ref,
+    outs_ref,
     normed_ref,
     full_ref,
-    decays_ref,
     norm_sent,
     norm_landed,
     side_sent,
@@ -265,6 +268,12 @@
     decay_sent,
     decay_landed,
     local_sem,
+    out_up_sent,
+    out_down_sent,
+    out_line_landed,
+    out_plane_sent,
+    out_plane_landed,
+    out_relay_sent,
 ):
     s, f, t = lax.axis_index("sp"), lax.axis_index("fs"), lax.axis_index("tp")
     xn, yn, dn = plane_partners(f)
@@ -283,6 +292,9 @@
     def own(piece):
         return half_ref.at[pl.ds(piece * chunk, chunk), :]
 
+    def outs(b, g):
+        return outs_ref.at[pl.ds((b * n_fs + g) * rows, rows), :]
+
     def block(b, g):
         return full_ref.at[pl.ds((b * n_fs + g) * rows, rows), :]
 
@@ -316,7 +328,25 @@
         def _():
             line_copy(source, b, g, -1).start()
 
+    def out_line(source, b, way):
+        sent = out_up_sent if way == 1 else out_down_sent
+        return remote(source, outs(b, f), sent.at[b], out_line_landed.at[b], {"sp": s + way})
+
+    def out_plane(source, b, i):
+        return remote(
+            source, outs(b, f), out_plane_sent.at[b, i], out_plane_landed.at[b, f], {"fs": order[i]}
+        )
+
     send_line(weight_ref.at[f], s, f)
+
+    @pl.when(s < n_sp - 1)
+    def _():
+        out_line(out_ref, s, 1).start()
+
+    @pl.when(s > 0)
+    def _():
+        out_line(out_ref, s, -1).start()
+
     for piece in range(2):
         start(remote(own(piece), spot(f, t, piece), side_sent.at[f, piece], side_landed.at[f, piece], other))
     for i, (a, b) in enumerate(
@@ -325,6 +355,7 @@
             (own(1), spot(f, t, 1)),
             (weight_ref.at[f], block(s, f)),
             (decay_ref.at[f], decays_ref.at[f]),
+            (out_ref, outs(s, f)),
         )
     ):
         copy = pltpu.make_async_copy(a, b, local_sem.at[i])
@@ -335,6 +366,9 @@
         remote(weight_ref.at[p], block(s, p), weight_sent.at[0], weight_landed.at[p], {"fs": p}).wait_recv()
         send_line(block(s, p), s, p)
 
+    for i in range(2):
+        out_plane(out_ref, s, i).start()
+
     def arrived(owner, piece):
         view = spot(owner, t, piece)
         remote(view, view, norm_sent.at[0], norm_landed.at[owner, piece], {"fs": owner}).wait_recv()
@@ -358,30 +392,86 @@
                 @pl.when(s > 0)
                 def _():
                     line_copy(block(s + d, g), s + d, g, -1).start()
+
+    def out_step(d):
+        for b, way, there, further in (
+            (s - d, 1, s - d >= 0, s < n_sp - 1),
+            (s + d, -1, s + d <= n_sp - 1, s > 0),
+        ):
+
+            @pl.when(there)
+            def _():
+                out_line(outs(b, f), b, way).wait_recv()
+
+                @pl.when(further)
+                def _():
+                    out_line(outs(b, f), b, way).start()
+
+                for i in range(2):
+                    out_plane(outs(b, f), b, i).start()
 
     arrived(xn, 0)
     start(remote(spot(xn, t, 0), spot(xn, t, 0), relay_sent.at[0], norm_landed.at[xn, 0], {"fs": yn}))
     arrived(yn, 1)
     start(remote(spot(yn, t, 1), spot(yn, t, 1), relay_sent.at[1], norm_landed.at[yn, 1], {"fs": xn}))
     line_step(1)
+    out_step(1)
     arrived(xn, 1)
     arrived(yn, 0)
     for d in range(2, n_sp - 1):
         line_step(d)
+        out_step(d)
     arrived(dn, 0)
     arrived(dn, 1)
     if n_sp > 2:
         line_step(n_sp - 1)
+        out_step(n_sp - 1)
     for p in order:
         remote(decay_ref.at[p], decays_ref.at[p], decay_sent.at[0], decay_landed.at[p], {"fs": p}).wait_recv()
     for owner in range(n_fs):
         for piece in range(2):
             view = spot(owner, 1 - t, piece)
             remote(view, view, side_sent.at[0, 0], side_landed.at[owner, piece], other).wait_recv()
+    for copy in locals_:
+        copy.wait()
+
+    def out_landed(b, g):
+        remote(outs(b, g), outs(b, g), out_relay_sent.at[0], out_plane_landed.at[b, g], {"fs": g}).wait_recv()
+
+    for b in range(n_sp):
+        g, onward = (xn, yn) if b < n_sp // 2 else (yn, xn)
+        out_landed(b, g)
+        start(
+            remote(outs(b, g), outs(b, g), out_relay_sent.at[b], out_plane_landed.at[b, g], {"fs": onward})
+        )
+
+    tile = chunk
+    tiles = 2 * half // tile
+
+    @pl.loop(0, n_fs * tiles)
+    def _(step):
+        owner, at = step // tiles, pl.ds((step % tiles) * tile, tile)
+        proj_ref[owner, at, :] = jnp.dot(
+            normed_ref[owner, at, :], full_ref[...], preferred_element_type=jnp.float32
+        ).astype(jnp.bfloat16)
+
+    for b in range(n_sp):
+        out_landed(b, yn if b < n_sp // 2 else xn)
+        out_landed(b, dn)
     for copy in waits:
         copy.wait_send()
-    for copy in locals_:
-        copy.wait()
+    for b in range(n_sp):
+        for i in range(2):
+            out_plane(outs(b, f), b, i).wait_send()
+
+        @pl.when((s < n_sp - 1) & (b <= s))
+        def _():
+            out_line(outs(b, f), b, 1).wait_send()
+
+        @pl.when((s > 0) & (b >= s))
+        def _():
+            out_line(outs(b, f), b, -1).wait_send()
+
     for b in range(n_sp):
         for g in range(n_fs):
 
@@ -394,7 +484,7 @@
                 line_copy(block(b, g), b, g, -1).wait_send()
 
 
-def gather_all(n_sp, half, pieces, decays):
+def gather_all(n_sp, half, pieces, decays, own_out):
     n_fs, rows, width = pieces.shape
     any_space = pl.BlockSpec(memory_space=pl.ANY)
     vmem = pl.BlockSpec(memory_space=pltpu.VMEM)
@@ -402,13 +492,15 @@
     return pl.pallas_call(
         lambda *refs: gather_kernel(n_sp, *refs),
         out_shape=(
-            jax.ShapeDtypeStruct((n_fs, 2 * half.shape[0], half.shape[1]), jnp.bfloat16),
-            jax.ShapeDtypeStruct((n_sp * n_fs * rows, width), jnp.bfloat16),
+            jax.ShapeDtypeStruct((n_fs, 2 * half.shape[0], width), jnp.bfloat16),
             jax.ShapeDtypeStruct(decays.shape, jnp.float32),
+            jax.ShapeDtypeStruct((n_sp * n_fs * rows, own_out.shape[1]), jnp.bfloat16),
         ),
-        in_specs=[vmem] * 3,
-        out_specs=(any_space, any_space, vmem),
+        in_specs=[vmem] * 4,
+        out_specs=(vmem, vmem, any_space),
         scratch_shapes=[
+            pltpu.VMEM((n_fs, 2 * half.shape[0], half.shape[1]), jnp.bfloat16),
+            pltpu.VMEM((n_sp * n_fs * rows, width), jnp.bfloat16),
             dma((4,)),
             dma((n_fs, 2)),
             dma((n_fs, 2)),
@@ -421,12 +513,18 @@
             dma((n_sp, n_fs)),
             dma((3,)),
             dma((n_fs,)),
-            dma((4,)),
+            dma((5,)),
+            dma((n_sp,)),
+            dma((n_sp,)),
+            dma((n_sp,)),
+            dma((n_sp, 2)),
+            dma((n_sp, n_fs)),
+            dma((n_sp,)),
         ],
         compiler_params=pltpu.CompilerParams(collective_id=0, has_side_effects=True),
         cost_estimate=pl.CostEstimate(flops=0, bytes_accessed=200_000_000, transcendentals=0),
         name="gather_all",
-    )(half, pieces, decays)
+    )(half, pieces, decays, own_out)
 
 
 def swap_kernel(
@@ -488,6 +586,63 @@
         cost_estimate=pl.CostEstimate(flops=0, bytes_accessed=60_000_000, transcendentals=0),
         name="swap",
     )(mixed, weight)
+
+
+def pass_kernel(n_sp, state_ref, extra_ref, states_ref, extras_ref, sent, landed, local_sem):
+    s = lax.axis_index("sp")
+    greet([{"sp": (s + d) % n_sp} for d in range(1, n_sp)])
+
+    def pair(source, here, owner, d):
+        place = here.at[owner]
+        slot = 0 if source is state_ref else 1
+        return remote(source, place, sent.at[d, slot], landed.at[owner, slot], {"sp": (s + d) % n_sp})
+
+    arrays = ((state_ref, states_ref), (extra_ref, extras_ref))
+    for d in range(n_sp - 1, 0, -1):
+
+        @pl.when(s + d < n_sp)
+        def _():
+            for source, here in arrays:
+                pair(source, here, s, d).start()
+
+    states_ref[n_sp - 1] = jnp.zeros_like(state_ref)
+    extras_ref[n_sp - 1] = jnp.zeros_like(extra_ref)
+    for k in range(n_sp - 1):
+
+        @pl.when(k < s)
+        def _():
+            for source, here in arrays:
+                pair(source, here, k, 1).wait_recv()
+
+        @pl.when(k >= s)
+        def _():
+            states_ref[k] = jnp.zeros_like(state_ref)
+            extras_ref[k] = jnp.zeros_like(extra_ref)
+
+    for d in range(1, n_sp):
+
+        @pl.when(s + d < n_sp)
+        def _():
+            for source, here in arrays:
+                pair(source, here, s, d).wait_send()
+
+
+def pass_on(n_sp, state, extra):
+    vmem = pl.BlockSpec(memory_space=pltpu.VMEM)
+    dma = pltpu.SemaphoreType.DMA
+    return pl.pallas_call(
+        lambda *refs: pass_kernel(n_sp, *refs),
+        out_shape=(
+            jax.ShapeDtypeStruct((n_sp,) + state.shape, state.dtype),
+            jax.ShapeDtypeStruct((n_sp,) + extra.shape, extra.dtype),
+        ),
+        in_specs=[vmem] * 2,
+        out_specs=(vmem, vmem),
+        scratch_shapes=[dma((n_sp, 2)), dma((n_sp, 2)), dma],
+        compiler_params=pltpu.CompilerParams(collective_id=2, has_side_effects=True),
+        cost_estimate=pl.CostEstimate(flops=0, bytes_accessed=20_000_000, transcendentals=0),
+        name="pass_on",
+    )(state, extra)
 
 
 def rotate_flat(values, cosine, sine):
@@ -538,14 +693,9 @@
         axis=-1,
     )
     own_out = jnp.concatenate([out_ret_weight, out_conv_weight], axis=-1)
-    out_weight = lax.all_gather(own_out, ("sp", "fs"), axis=0, tiled=True)
-    everyone, weights, decays = gather_all(
-        n_sp, normed, pieces, log_decay[0].reshape(n_fs, blocks, BLOCK_LEN)
-    )
-    proj = jnp.dot(
-        everyone.reshape(n_fs * tok_rows, model), weights, preferred_element_type=jnp.float32
-    ).astype(jnp.bfloat16)
-    proj = proj.reshape(n_fs, tok_rows, weights.shape[1])
+    proj, decays, out_weight = gather_all(
+        n_sp, normed, pieces, log_decay[0].reshape(n_fs, blocks, BLOCK_LEN), own_out
+    )
     cuts = (KEY_DIM, 2 * KEY_DIM)
     q_raw, k_raw, wide = proj[..., : cuts[0]], proj[..., cuts[0] : cuts[1]], proj[..., cuts[1] :]
     values, ret_gate, gate_b, gate_c, conv_in = jnp.split(wide, 5, axis=-1)
@@ -582,21 +732,20 @@
         start = start + ending[:, n]
     product = gate_c.astype(jnp.float32) * conv_in.astype(jnp.float32)
     halo = CONV_TAPS - 1
-    packed = jnp.concatenate(
+    extra = jnp.concatenate(
         [
-            state,
             product[:, tok_rows - halo :],
-            jnp.broadcast_to(start[..., None], (n_fs, 8 - halo, state.shape[-1])),
+            jnp.broadcast_to(start[..., None], (n_fs, 8 - halo, product.shape[-1])),
         ],
         axis=1,
     )
-    shared = lax.all_gather(packed, "sp")
+    all_states, extras = pass_on(n_sp, state.astype(jnp.bfloat16), extra)
     state_in = jnp.zeros_like(state)
     rim = jnp.zeros_like(product[:, :halo])
     for k in range(n_sp - 1):
-        part, total = shared[k, :, :KEY_DIM], shared[k, :, KEY_DIM + halo :][:, :1, :1]
+        part, total = all_states[k].astype(jnp.float32), extras[k, :, halo : halo + 1, :1]
         state_in = jnp.where(k < s, state_in * jnp.exp(total) + part, state_in)
-        rim = jnp.where(k == s - 1, shared[k, :, KEY_DIM : KEY_DIM + halo], rim)
+        rim = jnp.where(k == s - 1, extras[k, :, :halo], rim)
 
     raw = jnp.einsum("bnid,bnjd->bnij", queries, keys, preferred_element_type=jnp.float32)
     scores = (raw * weighting).astype(jnp.bfloat16)

time: 230 us -> 207 us (0.900)
  blocking collectives: 16.5 us -> 0 us
  between operations: 14 us -> 0.42 us
  matrix products: 29.9 us -> 19.5 us
  Pallas kernels: 129 us -> 138 us
  other arithmetic: 25.9 us -> 30.5 us
  local copies, waits for them, and re-layouts: 14.6 us -> 17 us
    all_gather x1 -> x0, blocking collectives: 16.5 us -> none  [fast_shards(): shared = lax.all_gather(packed, 'sp')]
    dot_general x1 -> x0, matrix products: 15.3 us -> none  [fast_shards(): jnp.dot(everyone.reshape(n_fs * tok_rows, model), weights, preferred_elem...]
    pallas_call x0 -> x1, Pallas kernels: none -> 6.55 us  [pass_on(): pl.pallas_call(lambda *refs: pass_kernel(n_sp, *refs), out_shape=(jax.Sha...]
    dot_general x2, matrix products: 7.3 us -> 12 us  [project(): lax.dot_general(spread(piece), weight, (((1,), (1,)), ((), ())), preferre...]
  transfers between devices with their start and end apart: 1 -> 0, of which waited for: 0 -> 0; matrix products, arithmetic and copies ran while one was open for 25% -> 0% of each run, Pallas kernels for 46% -> 0%
where the time goes in v2:
time: 207 us; the launch traced here: 206 us
  Pallas kernels  138 us (67%)
  other arithmetic  30.5 us (15%)
  matrix products  19.5 us (9%)
  local copies, waits for them, and re-layouts  17 us (8%)
    pallas_call x1, Pallas kernels, gather_all(): pl.pallas_call(lambda *refs: gather_kernel(n_sp, *refs), out_shape=(jax.S...  108 us
    pallas_call x1, Pallas kernels, swap(): pl.pallas_call(swap_kernel, out_shape=(piece, piece, jax.ShapeDtypeStruct...  23.5 us
    dot_general x2, matrix products, project(): lax.dot_general(spread(piece), weight, (((1,), (1,)), ((), ())), preferre...  12 us
    pallas_call x1, Pallas kernels, pass_on(): pl.pallas_call(lambda *refs: pass_kernel(n_sp, *refs), out_shape=(jax.Sha...  6.55 us
    another operation x1, other arithmetic  5.12 us
    concatenate x4, local copies, waits for them, and re-layouts, rotate_flat(): jnp.concatenate([first * cosine - second * sine, first * sine + second *...  5 us
    dot_general x1, matrix products, fast_shards(): jnp.einsum('bnij,bnje->bnie', scores, value_blocks, preferred_element_typ...  4.37 us

profile of v2, /device:TPU:0, one launch (start us, length us, event | category | flops | bytes accessed | tf_op | source)
XLA Modules:
  0.0 205.6 jit_solution(7047235231887003056)
XLA Ops:
  0.0 1.8 fusion
  1.9 3.1 %fusion.2.refs_0_ = bf16[384,2048]{1,0:T(8,128)(2,1)} fusion(f32[2048]{0:T(1024)S(1)} %copy-done.20, f32[384]{0:T(512)S(1)} %add_rsqrt_fusion.1, bf16[1,768,2048]{2,1,0:T(8,128)(2,1)} %param.13, s32[]{:T(128)S(6)} %select_n.67), kind=kLoop, calls=%fused_computation.4 | loop fusion | flops 3145728 | bytes 3155460 | tf_op jit(solution)/shard_map/convert_element_type | solution.py:679
  6.9 1.2 concatenate.46.refs_1_
  9.4 108.1 %gather_all.1 = (bf16[4,768,768]{2,1,0:T(8,128)(2,1)}, f32[4,6,128]{2,1,0:T(8,128)}, bf16[2048,1024]{1,0:T(8,128)(2,1)}) custom-call(bf16[384,2048]{1,0:T(8,128)(2,1)} %fusion.2.refs_0_, bf16[4,128,768]{2,1,0:T(8,128)(2,1)} %concatenate.46.refs_1_, f32[4,6,128]{2,1,0:T(8,128)} %reshape_squeeze.3.refs_2_, bf16[128,1024]{1,0:T(8,128)(2,1)} %pad_maximum_fusion.3.refs_3_), custom_call_target="tpu_custom_call" | custom-call | bytes 200000000 | tf_op jit(solution)/shard_map/gather_all/pallas_call | solution.py:492
  117.5 2.2 %reduce_window_sum.11 = f32[4,6,128]{2,1,0:T(8,128)S(1)} reduce-window(f32[4,6,128]{2,1,0:T(8,128)} %get-tuple-element.14, f32[]{:T(128)} %constant.23.clone.1), window={size=1x1x128 pad=0_0x0_0x127_0}, to_apply=%region_1.2 | reduce-window | flops 390144 | bytes 24580 | tf_op jit(solution)/shard_map/jit(cumsum)/reduce_window_sum | solution.py:714
  120.7 1.4 multiply_cosine_fusion
  122.1 5.1 %fusion.11 = (bf16[4,768,32]{2,1,0:T(8,128)(2,1)}, bf16[4,768,32]{2,1,0:T(8,128)(2,1)}, f32[4,768,32]{2,1,0:T(8,128)S(1)}, f32[4,768,32]{2,1,0:T(8,128)S(1)}) fusion(f32[768,32]{1,0:T(8,128)S(1)} %get-tuple-element.51, f32[768,32]{1,0:T(8,128)S(1)} %get-tuple-element.50, bf16[4,768,768]{2,1,0:T(8,128)(2,1)} %get-tuple-element.13), kind=kLoop, calls=%fused_computation.26 | loop fusion | flops 1769472 | bytes 2162688 | tf_op jit(solution)/shard_map/convert.7
  127.2 2.1 %copy.40 = bf16[4,6,128,32]{2,3,1,0:T(8,128)(2,1)} copy(bf16[4,6,128,32]{3,2,1,0:T(8,128)(2,1)} %bitcast.101) | data formatting | bytes 393216 | tf_op jit(solution)/shard_map/concatenate | solution.py:652
  129.3 2.1 %copy.39 = bf16[4,6,128,32]{2,3,1,0:T(8,128)(2,1)} copy(bf16[4,6,128,32]{3,2,1,0:T(8,128)(2,1)} %bitcast.100) | data formatting | bytes 393216 | tf_op jit(solution)/shard_map/concatenate | solution.py:652
  132.0 2.1 %split.15 = bf16[4,768,128]{2,1,0:T(8,128)(2,1)} slice(bf16[4,768,768]{2,1,0:T(8,128)(2,1)} %get-tuple-element.13), slice={[0:4], [0:768], [128:256]} | slice | bytes 1572864 | tf_op jit(solution)/shard_map/split | solution.py:701
  137.8 0.9 fusion.34.refs_0_
  138.8 1.6 convert_multiply_fusion.11
  141.0 6.5 %pass_on.1 = (bf16[4,4,64,128]{3,2,1,0:T(8,128)(2,1)}, f32[4,4,8,128]{3,2,1,0:T(8,128)}) custom-call(bf16[4,64,128]{2,1,0:T(8,128)(2,1)} %fusion.34.refs_0_, f32[4,8,128]{2,1,0:T(8,128)} %pad_maximum_fusion.7.refs_1_), custom_call_target="tpu_custom_call" | custom-call | bytes 20000000 | tf_op jit(solution)/shard_map/pass_on/pallas_call | solution.py:633
  147.5 1.4 multiply_reduce_fusion.1
  148.9 1.7 fusion.35
  151.3 2.8 %fusion.29 = f32[4,6,128,128]{3,2,1,0:T(8,128)} fusion(f32[4,6,128]{2,1,0:T(8,128)} %get-tuple-element.48, bf16[4,6,128,32]{2,3,1,0:T(8,128)(2,1)S(1)} %copy-done.5, bf16[4,6,128,32]{2,3,1,0:T(8,128)(2,1)S(1)} %copy-done.6, f32[4,6,64,128]{3,2,0,1:T(8,128)} %copy-done.3, f32[4,64,128]{2,1,0:T(8,128)} %fusion.35, f32[4,6]{0,1:T(8,128)S(1)} %exp.105), kind=kOutput, calls=%fused_computation.57 | convolution fusion | flops 52101120 | bytes 2895968 | tf_op jit(solution)/shard_map/bnid,bnde->bnie/dot_general | solution.py:759
  154.8 4.4 %multiply_reduce_fusion = (f32[4,6,128]{2,1,0:T(8,128)}, f32[4,6,128,128]{3,2,1,0:T(8,128)}) fusion(f32[4,6,128,128]{3,2,1,0:T(8,128)} %fusion.29, bf16[4,6,128,128]{3,2,1,0:T(8,128)(2,1)S(1)} %bitcast.103, f32[4,6,128]{2,1,0:T(8,128)} %copy-done.7, pred[128,128]{1,0:T(8,128)(4,1)} %iota_compare_fusion, bf16[4,6,128,32]{2,3,1,0:T(8,128)(2,1)S(1)} %copy-done.5, ...), kind=kOutput, calls=%fused_computation.38 | convolution fusion | flops 155513856 | bytes 5152768 | tf_op jit(solution)/shard_map/bnij,bnje->bnie/dot_general | solution.py:752
  159.9 1.9 broadcast_multiply_fusion
  162.6 2.5 %fusion.21 = (bf16[4,768,128]{2,1,0:T(8,128)(2,1)S(1)}, bf16[4,768,128]{2,1,0:T(8,128)(2,1)S(1)}) fusion(f32[4,6,128,128]{3,2,1,0:T(8,128)S(1)} %broadcast_multiply_fusion, bf16[4,768,768]{2,1,0:T(8,128)(2,1)} %get-tuple-element.13, f32[4,768,128]{2,1,0:T(8,128)S(1)} %convert_multiply_fusion.11, f32[128]{0:T(128)S(1)} %get-tuple-element.53, ...), kind=kLoop, calls=%fused_computation.41 | loop fusion | flops 6684672 | bytes 6297088 | tf_op jit(solution)/shard_map/convert_element_type | solution.py:768
  165.1 1.3 pad_maximum_fusion.1.mixed_ref
  166.4 23.5 %swap.1 = (bf16[4,384,256]{2,1,0:T(8,128)(2,1)}, bf16[4,384,256]{2,1,0:T(8,128)(2,1)}, bf16[2048,1024]{1,0:T(8,128)(2,1)}) custom-call(bf16[4,768,256]{2,1,0:T(8,128)(2,1)} %pad_maximum_fusion.1.mixed_ref, bf16[2048,1024]{1,0:T(8,128)(2,1)} %get-tuple-element.17.weight_ref), custom_call_target="tpu_custom_call" | custom-call | bytes 60000000 | tf_op jit(solution)/shard_map/swap/pallas_call | solution.py:579
  189.9 2.0 reshape.345
  192.7 5.8 %fusion.61 = f32[384,2048]{1,0:T(8,128)} fusion(bf16[384,1024]{0,1:T(8,128)(2,1)S(1)} %bitcast.105, bf16[2048,1024]{1,0:T(8,128)(2,1)} %get-tuple-element.17.weight_ref), kind=kOutput, calls=%fused_computation.131 | convolution fusion | flops 1610612736 | bytes 8126464 | tf_op jit(solution)/shard_map/dot_general | solution.py:783
  199.4 6.2 %fusion.3 = bf16[1,384,2048]{2,1,0:T(8,128)(2,1)} fusion(f32[384,2048]{1,0:T(8,128)} %fusion.61, bf16[384,1024]{0,1:T(8,128)(2,1)S(1)} %bitcast.104, bf16[2048,1024]{1,0:T(8,128)(2,1)} %get-tuple-element.20), kind=kOutput, calls=%fused_computation.6 | convolution fusion | flops 1612185600 | bytes 9699328 | tf_op jit(solution)/shard_map/dot_general | solution.py:783
  (89 shorter events, 13.5 us)
Async XLA Ops:
  0.0 161.7 %copy-start = (f32[3,512]{1,0:T(4,128)S(1)}, f32[3,512]{1,0:T(4,128)}, u32[]{:S(2)}) copy-start(f32[3,512]{1,0:T(4,128)} %param.22) | copy-start | bytes 18436
  0.0 1.8 copy-start.20
  1.8 3.1 %copy-start.17 = (bf16[128,256]{1,0:T(8,128)(2,1)S(1)}, bf16[128,256]{1,0:T(8,128)(2,1)}, u32[]{:S(2)}) copy-start(bf16[128,256]{1,0:T(8,128)(2,1)} %param.15) | copy-start | bytes 196612
  1.9 3.4 %copy-start.18 = (bf16[128,256]{1,0:T(8,128)(2,1)S(1)}, bf16[128,256]{1,0:T(8,128)(2,1)}, u32[]{:S(2)}) copy-start(bf16[128,256]{1,0:T(8,128)(2,1)} %param.16) | copy-start | bytes 196612
  1.9 3.6 %copy-start.9 = (bf16[128,512]{1,0:T(8,128)(2,1)S(1)}, bf16[128,512]{1,0:T(8,128)(2,1)}, u32[]{:S(2)}) copy-start(bf16[128,512]{1,0:T(8,128)(2,1)} %param.17) | copy-start | bytes 393220
  1.9 3.9 %copy-start.10 = (bf16[128,512]{1,0:T(8,128)(2,1)S(1)}, bf16[128,512]{1,0:T(8,128)(2,1)}, u32[]{:S(2)}) copy-start(bf16[128,512]{1,0:T(8,128)(2,1)} %param.18) | copy-start | bytes 393220
  4.9 1.1 copy-start.11
  4.9 1.4 copy-start.12
  4.9 1.7 copy-start.13
  6.2 1.9 copy-start.19
  6.2 2.5 %copy-start.14 = (bf16[128,512]{1,0:T(8,128)(2,1)S(1)}, bf16[128,512]{1,0:T(8,128)(2,1)}, u32[]{:S(2)}) copy-start(bf16[128,512]{1,0:T(8,128)(2,1)} %param.24) | copy-start | bytes 393220
  6.2 2.5 %copy-start.15 = (bf16[128,512]{1,0:T(8,128)(2,1)S(1)}, bf16[128,512]{1,0:T(8,128)(2,1)}, u32[]{:S(2)}) copy-start(bf16[128,512]{1,0:T(8,128)(2,1)} %param.23) | copy-start | bytes 393220
  119.7 2.4 %copy-start.7 = (f32[4,6,128]{2,1,0:T(8,128)}, f32[4,6,128]{2,1,0:T(8,128)S(1)}, u32[]{:S(2)}) copy-start(f32[4,6,128]{2,1,0:T(8,128)S(1)} %reduce_window_sum.11) | copy-start | bytes 36868
  134.5 1.1 copy-start.1
  134.5 1.1 copy-start.16
  135.7 0.7 copy-start.8
  135.7 1.6 copy-start.2
  137.8 2.6 %copy-start.3 = (f32[4,6,64,128]{3,2,0,1:T(8,128)}, f32[4,6,64,128]{3,2,0,1:T(8,128)S(1)}, u32[]{:S(2)}) copy-start(f32[4,6,64,128]{3,2,0,1:T(8,128)S(1)} %add_dynamic-update-slice_fusion) | copy-start | bytes 2359300
  138.7 12.6 %copy-start.5 = (bf16[4,6,128,32]{2,3,1,0:T(8,128)(2,1)S(1)}, bf16[4,6,128,32]{2,3,1,0:T(8,128)(2,1)}, u32[]{:S(2)}) copy-start(bf16[4,6,128,32]{2,3,1,0:T(8,128)(2,1)} %copy.40) | copy-start | bytes 589828
  138.8 12.6 %copy-start.6 = (bf16[4,6,128,32]{2,3,1,0:T(8,128)(2,1)S(1)}, bf16[4,6,128,32]{2,3,1,0:T(8,128)(2,1)}, u32[]{:S(2)}) copy-start(bf16[4,6,128,32]{2,3,1,0:T(8,128)(2,1)} %copy.39) | copy-start | bytes 589828
  192.7 5.8 %copy-start.4 = (bf16[4,384,256]{2,1,0:T(8,128)(2,1)S(1)}, bf16[4,384,256]{2,1,0:T(8,128)(2,1)}, u32[]{:S(2)}) copy-start(bf16[4,384,256]{2,1,0:T(8,128)(2,1)} %get-tuple-element.19) | copy-start | bytes 2359300
